TPU v7x, 32 devices: a whole 2x2x4 slice. The times are simulated.
32 devices in a mesh: ep: 8 (over z, core), tp: 4 (over y, x).
Axes of the slice: x: 2, y: 2, z: 4, core: 2. Of those that a mesh axis runs over, the one named last changes fastest.
Arguments:
- tokens: bfloat16 [128, 2048], P('ep'), may hold values from -6 to 6
- attn_gain: float32 [2048], replicated, may hold values from 0.1 to 1.9
- query_weight: bfloat16 [2048, 2048], P('ep', 'tp'), may hold values from -0.125 to 0.125
- key_weight: bfloat16 [2048, 2048], P('ep', 'tp'), may hold values from -0.125 to 0.125
- value_weight: bfloat16 [2048, 2048], P('ep', 'tp'), may hold values from -0.125 to 0.125
- forget_weight: bfloat16 [2048, 16], P(None, 'tp'), may hold values from -0.125 to 0.125
- forget_bias: float32 [16], P('tp'), may hold values from -1 to 2
- cache_keys: bfloat16 [128, 16, 384, 128], P('ep', 'tp'), may hold values from -240 to 240
- cache_values: bfloat16 [128, 16, 384, 128], P('ep', 'tp'), may hold values from -6 to 6
- cache_gates: float32 [128, 16, 384], P('ep', 'tp'), may hold values from -768 to 0, as said below
- lengths: int32 [128], P('ep'), may hold values from 1 to 384
- output_weight: bfloat16 [2048, 2048], P('tp', 'ep'), may hold values from -0.125 to 0.125
- ffn_gain: float32 [2048], replicated, may hold values from 0.1 to 1.9
- dense_gate_proj: bfloat16 [2048, 2048], P('ep', 'tp'), may hold values from -0.125 to 0.125
- dense_up_proj: bfloat16 [2048, 2048], P('ep', 'tp'), may hold values from -0.125 to 0.125
- dense_down_proj: bfloat16 [2048, 2048], P('tp', 'ep'), may hold values from -0.125 to 0.125
- dense_mix: bfloat16 [2048], replicated, may hold values from -0.125 to 0.125
- expert_ids: int32 [128, 2], P('ep'), may hold values from 0 to 7, as said below
- group_prob: float32 [128], P('ep'), may hold values from 0.25 to 1
- pair_prob: float32 [128, 2], P('ep'), may hold values from 0.05 to 1
- expert_gate: bfloat16 [8, 2048, 2048], P('ep', None, 'tp'), may hold values from -0.125 to 0.125
- expert_up: bfloat16 [8, 2048, 2048], P('ep', None, 'tp'), may hold values from -0.125 to 0.125
- expert_down: bfloat16 [8, 2048, 2048], P('ep', 'tp'), may hold values from -0.125 to 0.125
Outputs:
- mixed_out: bfloat16 [128, 2048], P('ep')
Inputs may be any that keep to these rules, and one draw needn't show every extreme that they name: `expert_ids`: each row names two different experts of one group, the groups being 4 runs of consecutive ids. In each aligned block of 16 rows (the rows of one index of ep) no expert is named more than 8 times, and some expert exactly 8 times. `cache_gates`: along positions the values never rise.
All inputs are finite; a program needn't handle non-finite values.
Results may differ from a plain program's by a relative error of at most 0.014.
Values may be sent and summed in bfloat16 or wider, within the bound.
A program may use at most 64 MiB of HBM per device.

v0:
```python
import math
import jax
import jax.numpy as jnp
from jax import lax
from jax.sharding import PartitionSpec as P

EPSILON = 1e-06


def rms_scale(values, norm_gain):
    widened = values.astype(jnp.float32)
    return (
        widened
        * lax.rsqrt(jnp.mean(widened * widened, axis=-1, keepdims=True) + EPSILON)
        * norm_gain
    )


def attend(queries, keys_new, values_new, key_cache, value_cache, gate_cache, lengths, log_forget):
    cache_span = key_cache.shape[2]
    score_scale = 1.0 / math.sqrt(key_cache.shape[3])
    positions = jnp.arange(cache_span, dtype=jnp.int32)
    live_mask = positions[None, :] < lengths[:, None]
    last_mask = positions[None, :] == lengths[:, None] - 1
    last_gate = jnp.sum(jnp.where(last_mask[:, None, :], gate_cache, 0.0), axis=-1)
    gate_now = last_gate + log_forget
    scores = (
        jnp.einsum("shd,shpd->shp", queries, key_cache, preferred_element_type=jnp.float32)
        * score_scale
    )
    scores = scores + gate_now[:, :, None] - gate_cache
    scores = jnp.where(live_mask[:, None, :], scores, -jnp.inf)
    own_score = (
        jnp.sum(queries.astype(jnp.float32) * keys_new.astype(jnp.float32), axis=-1) * score_scale
    )
    row_top = jnp.maximum(jnp.max(scores, axis=-1), own_score)
    raised = jnp.exp(scores - row_top[:, :, None])
    own_raised = jnp.exp(own_score - row_top)
    totals = jnp.sum(raised, axis=-1) + own_raised
    weights_low = (raised / totals[:, :, None]).astype(jnp.bfloat16)
    own_prob = (own_raised / totals).astype(jnp.bfloat16)
    attended = jnp.einsum(
        "shp,shpd->shd", weights_low, value_cache, preferred_element_type=jnp.float32
    )
    attended = attended + own_prob.astype(jnp.float32)[:, :, None] * values_new.astype(jnp.float32)
    return attended.astype(jnp.bfloat16)


def row_term(spread, joined):
    return jnp.dot(spread, joined, preferred_element_type=jnp.float32)


def right_product(left_rows, weight_piece):
    return jnp.dot(left_rows, weight_piece, preferred_element_type=jnp.float32)


def shards(
    tokens,
    attn_gain,
    query_weight,
    key_weight,
    value_weight,
    forget_weight,
    forget_bias,
    cache_keys,
    cache_values,
    cache_gates,
    lengths,
    output_weight,
    ffn_gain,
    dense_gate_proj,
    dense_up_proj,
    dense_down_proj,
    dense_mix,
    expert_ids,
    group_prob,
    pair_prob,
    expert_gate,
    expert_up,
    expert_down,
):
    seq_count = tokens.shape[0]
    head_count = cache_keys.shape[1]
    head_size = cache_keys.shape[3]
    proj_width = query_weight.shape[1]
    normed = rms_scale(tokens, attn_gain).astype(jnp.bfloat16)
    spread = lax.all_to_all(normed, "ep", split_axis=1, concat_axis=0, tiled=True)
    joined = jnp.concatenate([query_weight, key_weight, value_weight], axis=1)
    summed = lax.psum_scatter(row_term(spread, joined), "ep", scatter_dimension=0, tiled=True)
    projected = (
        summed[:, :proj_width],
        summed[:, proj_width : 2 * proj_width],
        summed[:, 2 * proj_width :],
    )
    queries = projected[0].astype(jnp.bfloat16).reshape(seq_count, head_count, head_size)
    keys_new = projected[1].astype(jnp.bfloat16).reshape(seq_count, head_count, head_size)
    values_new = projected[2].astype(jnp.bfloat16).reshape(seq_count, head_count, head_size)
    log_forget = jax.nn.log_sigmoid(
        jnp.dot(normed, forget_weight, preferred_element_type=jnp.float32) + forget_bias
    )
    attended = attend(
        queries, keys_new, values_new, cache_keys, cache_values, cache_gates, lengths, log_forget
    )
    attended = attended.reshape(seq_count, head_count * head_size)
    head_terms = right_product(attended, lax.all_gather(output_weight, "ep", axis=1, tiled=True))
    mixed_heads = lax.psum(head_terms, "tp")
    residual = (tokens.astype(jnp.float32) + mixed_heads).astype(jnp.bfloat16)
    ffn_in = rms_scale(residual, ffn_gain).astype(jnp.bfloat16)
    dense_width = dense_gate_proj.shape[1]
    ffn_spread = lax.all_to_all(ffn_in, "ep", split_axis=1, concat_axis=0, tiled=True)
    dense_joined = jnp.concatenate([dense_gate_proj, dense_up_proj], axis=1)
    dense_summed = lax.psum_scatter(
        row_term(ffn_spread, dense_joined).astype(jnp.bfloat16),
        "ep",
        scatter_dimension=0,
        tiled=True,
    ).astype(jnp.float32)
    dense_parts = (dense_summed[:, :dense_width], dense_summed[:, dense_width:])
    dense_hidden = (jax.nn.silu(dense_parts[0]) * dense_parts[1]).astype(jnp.bfloat16)
    dense_terms = right_product(
        dense_hidden, lax.all_gather(dense_down_proj, "ep", axis=1, tiled=True)
    )
    dense_total = lax.psum(dense_terms.astype(jnp.bfloat16), "tp").astype(jnp.float32)
    mix = jax.nn.sigmoid(jnp.dot(ffn_in, dense_mix, preferred_element_type=jnp.float32))
    expert_count = lax.axis_size("ep") * expert_gate.shape[0]
    capacity = 4 * seq_count // expert_count
    slot_total = expert_count * capacity
    picks = expert_ids.reshape(-1)
    expert_grid = jnp.arange(expert_count, dtype=jnp.int32)
    pick_onehot = (picks[:, None] == expert_grid[None, :]).astype(jnp.int32)
    earlier = jnp.cumsum(pick_onehot, axis=0) - pick_onehot
    slot_rank = jnp.sum(earlier * pick_onehot, axis=1)
    destination = (picks * capacity + slot_rank).reshape(seq_count, 2)
    slot_grid = jnp.arange(slot_total, dtype=jnp.int32)
    select_first = (destination[:, 0:1] == slot_grid[None, :]).astype(jnp.bfloat16)
    select_second = (destination[:, 1:2] == slot_grid[None, :]).astype(jnp.bfloat16)
    selector = select_first + select_second
    outbound = jnp.einsum("sk,sd->kd", selector, ffn_in, preferred_element_type=jnp.float32)
    outbound = outbound.astype(jnp.bfloat16).reshape(expert_count, capacity, ffn_in.shape[1])
    arrived = lax.all_to_all(outbound, "ep", split_axis=0, concat_axis=0, tiled=True)
    sources, slots_now, feature = arrived.shape
    row_data = arrived.reshape(sources * slots_now, feature)
    gate_part = jnp.dot(row_data, expert_gate[0], preferred_element_type=jnp.float32)
    up_part = jnp.dot(row_data, expert_up[0], preferred_element_type=jnp.float32)
    expert_hidden = (jax.nn.silu(gate_part) * up_part).astype(jnp.bfloat16)
    partial_out = jnp.dot(expert_hidden, expert_down[0], preferred_element_type=jnp.float32)
    expert_result = lax.psum(partial_out.astype(jnp.bfloat16), "tp").astype(jnp.float32)
    returned = lax.all_to_all(
        expert_result.reshape(sources, slots_now, feature).astype(jnp.bfloat16),
        "ep",
        split_axis=0,
        concat_axis=0,
        tiled=True,
    ).astype(jnp.float32)
    returned = returned.reshape(slot_total, ffn_in.shape[1])
    routes = group_prob[:, None] * pair_prob / jnp.sum(pair_prob, axis=1, keepdims=True)
    first_back = returned[destination[:, 0]]
    second_back = returned[destination[:, 1]]
    side_total = (
        routes[:, 0:1] * first_back + routes[:, 1:2] * second_back + mix[:, None] * dense_total
    )
    result = residual.astype(jnp.float32) + side_total
    return result.astype(jnp.bfloat16)


def solution(mesh):
    return jax.shard_map(
        shards,
        mesh=mesh,
        in_specs=(
            P("ep", None),
            P(),
            P("ep", "tp"),
            P("ep", "tp"),
            P("ep", "tp"),
            P(None, "tp"),
            P("tp"),
            P("ep", "tp", None, None),
            P("ep", "tp", None, None),
            P("ep", "tp", None),
            P("ep"),
            P("tp", "ep"),
            P(),
            P("ep", "tp"),
            P("ep", "tp"),
            P("tp", "ep"),
            P(),
            P("ep", None),
            P("ep"),
            P("ep", None),
            P("ep", None, "tp"),
            P("ep", None, "tp"),
            P("ep", "tp", None),
        ),
        out_specs=P("ep", None),
        check_vma=False,
    )
```

profile of v0, /device:TPU:0, one launch (start us, length us, event | category | flops | bytes accessed | tf_op | source)
XLA Modules:
  0.0 268.5 jit_solution(17298867801017753038)
XLA Ops:
  6.5 0.0 reduce-scatter.3.cloned.1.call-start
  6.6 1.1 fusion.32
  7.7 0.9 fusion.34
  8.7 12.1 %all_to_all.48 = bf16[16,8,256]{2,0,1:T(8,128)(2,1)S(1)} all-to-all(bf16[16,8,256]{2,0,1:T(8,128)(2,1)S(1)} %bitcast.96), channel_id=1, replica_groups=mesh['ep'=8,'tp'=4] {'ep'}, dimensions={1} | all-to-all | bytes 131072 | tf_op jit(solution)/shard_map/all_to_all | solution.py:87
  20.7 2.3 fusion.20
  23.0 0.0 reduce-scatter.3.cloned.1.call-update
  23.0 0.0 all-gather.3.cloned.1.call-start
  23.1 0.7 all-gather.3.cloned.1.call-update
  23.8 0.0 all-reduce.4.cloned.1.call-start
  23.8 0.0 copy-done.10
  23.9 0.1 iota_compare_fusion
  23.9 0.1 select_reduce_fusion
  24.0 0.1 copy.42
  24.1 0.0 copy-done.14
  24.1 0.1 fusion.70
  24.3 0.1 copy.43
  24.4 0.1 iota_compare_fusion.1
  24.4 29.2 %reduce-scatter.3.cloned.1.call-done = f32[16,1536]{1,0:T(8,128)} async-done(((f32[128,1536]{1,0:T(8,128)}), f32[16,1536]{1,0:T(8,128)}) %reduce-scatter.3.cloned.1.call-update) | async-done | bytes 98320 | tf_op jit(solution)/shard_map/reduce_scatter | solution.py:89
  53.6 0.9 convert.8
  54.6 0.1 multiply_reduce_fusion
  54.7 0.0 copy-start.1
  54.7 5.2 %fusion.80 = f32[16,4,1,384]{3,2,1,0:T(1,128)S(1)} fusion(bf16[16,4,128,1]{2,3,1,0:T(2,128)(2,1)S(1)} %reshape.151, bf16[16,4,384,128]{3,2,1,0:T(8,128)(2,1)} %param.30), kind=kOutput, calls=%fused_computation.117 | convolution fusion | flops 6291456 | bytes 6406144 | tf_op jit(solution)/shard_map/shd,shpd->shp/dot_general | solution.py:28
  59.9 0.2 fusion.78
  60.1 0.2 fusion.50
  60.3 0.1 fusion.52
  60.5 1.2 fusion.48
  61.7 0.0 copy-start.12
  61.7 0.1 add_convert_fusion
  61.8 22.4 %all-gather.3.cloned.1.call-done = bf16[512,2048]{1,0:T(8,128)(2,1)} async-done(((bf16[512,256]{1,0:T(8,128)(2,1)}), bf16[512,2048]{1,0:T(8,128)(2,1)}) %all-gather.3.cloned.1.call-update) | async-done | bytes 2097168 | tf_op jit(solution)/shard_map/all_gather | solution.py:105
  84.2 2.6 fusion.55
  86.8 0.0 all-reduce.4.cloned.1.call-update
  86.9 0.0 reduce-scatter.5.cloned.1.call-start
  86.9 41.4 %all-reduce.4.cloned.1.call-done = f32[16,2048]{1,0:T(8,128)} async-done(((f32[16,2048]{1,0:T(8,128)}), f32[16,2048]{1,0:T(8,128)}) %all-reduce.4.cloned.1.call-update) | async-done | bytes 131088 | tf_op jit(solution)/shard_map/psum | solution.py:106
  128.3 1.0 fusion.36
  129.4 0.1 fusion.38
  129.5 10.3 %all_to_all.49 = bf16[16,8,256]{2,0,1:T(8,128)(2,1)S(1)} all-to-all(bf16[16,8,256]{2,0,1:T(8,128)(2,1)S(1)} %bitcast.97), channel_id=1, replica_groups=mesh['ep'=8,'tp'=4] {'ep'}, dimensions={1} | all-to-all | bytes 131072 | tf_op jit(solution)/shard_map/all_to_all | solution.py:110
  139.8 0.9 convolution_convert_fusion.3
  140.8 0.0 reduce-scatter.5.cloned.1.call-update
  140.8 0.0 all-gather.5.cloned.1.call-start
  140.8 0.5 all-gather.5.cloned.1.call-update
  141.4 0.0 all-reduce.6.cloned.1.call-start
  141.4 0.1 copy.44
  141.5 0.1 eq.62
  141.6 0.1 fusion.59
  141.7 0.1 reduce_window_sum.11
  141.7 0.2 select_reduce_fusion.1
  141.9 0.1 reduce_sum.71
  142.0 0.1 copy.45
  142.1 0.3 fusion
  142.4 12.7 %all_to_all.50 = bf16[8,8,2048]{2,1,0:T(8,128)(2,1)S(1)} all-to-all(bf16[8,8,2048]{2,1,0:T(8,128)(2,1)S(1)} %fusion), channel_id=1, replica_groups=mesh['ep'=8,'tp'=4] {'ep'}, dimensions={0} | all-to-all | bytes 524288 | tf_op jit(solution)/shard_map/all_to_all | solution.py:140
  155.1 2.1 fusion.5
  157.2 3.2 %fusion.1 = bf16[8,8,2048]{2,1,0:T(8,128)(2,1)} fusion(bf16[1,512,2048]{2,1,0:T(8,128)(2,1)S(1)} %copy-done, bf16[1,2048,512]{2,1,0:T(8,128)(2,1)} %param.44, bf16[8,8,2048]{2,1,0:T(8,128)(2,1)S(1)} %all_to_all.50, f32[64,512]{1,0:T(8,128)S(1)} %fusion.5), kind=kOutput, calls=%fused_computation.5 | convolution fusion | flops 268763136 | bytes 4849664 | tf_op jit(solution)/shard_map/dot_general | solution.py:146
  160.5 9.1 %reduce-scatter.5.cloned.1.call-done = bf16[16,1024]{1,0:T(8,128)(2,1)} async-done(((bf16[128,1024]{1,0:T(8,128)(2,1)}), bf16[16,1024]{1,0:T(8,128)(2,1)}) %reduce-scatter.5.cloned.1.call-update) | async-done | bytes 32784 | tf_op jit(solution)/shard_map/reduce_scatter | solution.py:112
  169.6 0.8 convert_element_type.119
  170.3 29.4 %all-gather.5.cloned.1.call-done = bf16[512,2048]{1,0:T(8,128)(2,1)} async-done(((bf16[512,256]{1,0:T(8,128)(2,1)}), bf16[512,2048]{1,0:T(8,128)(2,1)}) %all-gather.5.cloned.1.call-update) | async-done | bytes 2097168 | tf_op jit(solution)/shard_map/all_gather | solution.py:121
  199.7 2.6 convolution_convert_fusion.2
  202.3 0.0 all-reduce.6.cloned.1.call-update
  202.4 42.8 %all-reduce.6.cloned.1.call-done = (bf16[16,2048]{1,0:T(8,128)(2,1)}, bf16[8,8,2048]{2,1,0:T(8,128)(2,1)}) async-done(((bf16[16,2048]{1,0:T(8,128)(2,1)}, bf16[8,8,2048]{2,1,0:T(8,128)(2,1)}), (bf16[16,2048]{1,0:T(8,128)(2,1)}, bf16[8,8,2048]{2,1,0:T(8,128)(2,1)})) %all-reduce.6.cloned.1.call-update) | async-done | bytes 327696 | tf_op jit(solution)/shard_map/psum | solution.py:123
  245.2 4.7 %all-to-all-start.2 = ((bf16[8,8,2048]{2,1,0:T(8,128)(2,1)}), bf16[8,8,2048]{2,1,0:T(8,128)(2,1)S(1)}, u32[]{:S(2)}, u32[]{:S(2)}) async-start(bf16[8,8,2048]{2,1,0:T(8,128)(2,1)} %get-tuple-element.6), calls=%async_computation.3 | async-start | bytes 524288 | tf_op jit(solution)/shard_map/all_to_all | solution.py:148
  250.0 0.1 fusion.17
  250.1 9.5 %all-to-all-done.2 = bf16[8,8,2048]{2,1,0:T(8,128)(2,1)S(1)} async-done(((bf16[8,8,2048]{2,1,0:T(8,128)(2,1)}), bf16[8,8,2048]{2,1,0:T(8,128)(2,1)S(1)}, u32[]{:S(2)}, u32[]{:S(2)}) %all-to-all-start.2) | async-done | bytes 262176 | tf_op jit(solution)/shard_map/all_to_all | solution.py:148
  259.7 0.6 gather_fusion
  260.3 0.6 gather_fusion.1
  260.9 0.7 fusion.39
  (46 shorter events, 0.3 us)
Async XLA Ops:
  6.5 150.7 %copy-start = (bf16[1,512,2048]{2,1,0:T(8,128)(2,1)S(1)}, bf16[1,512,2048]{2,1,0:T(8,128)(2,1)}, u32[]{:S(2)}) copy-start(bf16[1,512,2048]{2,1,0:T(8,128)(2,1)} %param.45) | copy-start | bytes 6291460
  6.5 17.3 %copy-start.10 = (s32[16]{0:T(128)S(1)}, s32[16]{0:T(128)}, u32[]{:S(2)}) copy-start(s32[16]{0:T(128)} %param.33) | copy-start | bytes 196
  6.5 17.4 %copy-start.3 = (f32[16,4,384]{2,1,0:T(4,128)S(1)}, f32[16,4,384]{2,1,0:T(4,128)}, u32[]{:S(2)}) copy-start(f32[16,4,384]{2,1,0:T(4,128)} %param.32) | copy-start | bytes 294916
  6.5 17.6 %copy-start.13 = (bf16[2048,4]{0,1:T(4,128)(2,1)S(1)}, bf16[2048,4]{0,1:T(4,128)(2,1)}, u32[]{:S(2)}) copy-start(bf16[2048,4]{0,1:T(4,128)(2,1)} %param.28) | copy-start | bytes 49156
  6.5 17.6 %copy-start.14 = (f32[4]{0:T(128)S(1)}, f32[4]{0:T(128)}, u32[]{:S(2)}) copy-start(f32[4]{0:T(128)} %param.29) | copy-start | bytes 52
  6.5 47.1 %reduce-scatter.3.cloned.1.call-start = ((), (), s32[]{:S(2)}) async-start(), calls=%async_computation.6 | async-start | bytes 884736 | tf_op jit(solution)/shard_map/reduce_scatter | solution.py:89
  23.0 61.2 %all-gather.3.cloned.1.call-start = ((), (), s32[]{:S(2)}) async-start(), calls=%async_computation.7 | async-start | bytes 2359296 | tf_op jit(solution)/shard_map/all_gather | solution.py:105
  23.8 104.6 %all-reduce.4.cloned.1.call-start = ((), (), s32[]{:S(2)}) async-start(), calls=%async_computation.8 | async-start | bytes 262144 | tf_op jit(solution)/shard_map/psum | solution.py:106
  54.7 5.8 %copy-start.1 = (bf16[16,4,384,128]{3,2,1,0:T(8,128)(2,1)S(1)}, bf16[16,4,384,128]{3,2,1,0:T(8,128)(2,1)}, u32[]{:S(2)}) copy-start(bf16[16,4,384,128]{3,2,1,0:T(8,128)(2,1)} %param.31) | copy-start | bytes 18874372
  61.7 66.7 %copy-start.2 = (bf16[16,2048]{1,0:T(8,128)(2,1)S(1)}, bf16[16,2048]{1,0:T(8,128)(2,1)}, u32[]{:S(2)}) copy-start(bf16[16,2048]{1,0:T(8,128)(2,1)} %param.23) | copy-start | bytes 196612
  61.7 67.7 %copy-start.5 = (f32[2048]{0:T(1024)S(1)}, f32[2048]{0:T(1024)}, u32[]{:S(2)}) copy-start(f32[2048]{0:T(1024)} %param.35) | copy-start | bytes 24580
  61.7 78.2 %copy-start.11 = (bf16[256,512]{1,0:T(8,128)(2,1)S(1)}, bf16[256,512]{1,0:T(8,128)(2,1)}, u32[]{:S(2)}) copy-start(bf16[256,512]{1,0:T(8,128)(2,1)} %param.37) | copy-start | bytes 786436
  61.7 78.1 %copy-start.12 = (bf16[256,512]{1,0:T(8,128)(2,1)S(1)}, bf16[256,512]{1,0:T(8,128)(2,1)}, u32[]{:S(2)}) copy-start(bf16[256,512]{1,0:T(8,128)(2,1)} %param.36) | copy-start | bytes 786436
  84.2 57.2 %copy-start.7 = (s32[16,2]{0,1:T(2,128)S(1)}, s32[16,2]{0,1:T(2,128)}, u32[]{:S(2)}) copy-start(s32[16,2]{0,1:T(2,128)} %param.40) | copy-start | bytes 388
  86.9 82.7 %reduce-scatter.5.cloned.1.call-start = ((), (), s32[]{:S(2)}) async-start(), calls=%async_computation.9 | async-start | bytes 294912 | tf_op jit(solution)/shard_map/reduce_scatter | solution.py:112
  140.8 58.9 %all-gather.5.cloned.1.call-start = ((), (), s32[]{:S(2)}) async-start(), calls=%async_computation.10 | async-start | bytes 2359296 | tf_op jit(solution)/shard_map/all_gather | solution.py:121
  141.4 103.8 %all-reduce.6.cloned.1.call-start = ((), (), s32[]{:S(2)}) async-start(), calls=%async_computation.11 | async-start | bytes 655360 | tf_op jit(solution)/shard_map/psum | solution.py:123
  160.4 41.9 %copy-start.8 = (f32[16,2]{0,1:T(2,128)S(1)}, f32[16,2]{0,1:T(2,128)}, u32[]{:S(2)}) copy-start(f32[16,2]{0,1:T(2,128)} %param.42) | copy-start | bytes 388
  160.4 41.9 %copy-start.9 = (f32[16]{0:T(128)S(1)}, f32[16]{0:T(128)}, u32[]{:S(2)}) copy-start(f32[16]{0:T(128)} %param.41) | copy-start | bytes 196
  160.4 89.5 %copy-start.6 = (bf16[2048]{0:T(1024)(128)(2,1)S(1)}, bf16[2048]{0:T(1024)(128)(2,1)}, u32[]{:S(2)}) copy-start(bf16[2048]{0:T(1024)(128)(2,1)} %param.39) | copy-start | bytes 12292
  245.2 15.7 %copy-start.4 = (bf16[16,2048]{1,0:T(8,128)(2,1)S(1)}, bf16[16,2048]{1,0:T(8,128)(2,1)}, u32[]{:S(2)}) copy-start(bf16[16,2048]{1,0:T(8,128)(2,1)} %get-tuple-element.5) | copy-start | bytes 196612
  245.2 14.4 %all-to-all-start.2 = ((bf16[8,8,2048]{2,1,0:T(8,128)(2,1)}), bf16[8,8,2048]{2,1,0:T(8,128)(2,1)S(1)}, u32[]{:S(2)}, u32[]{:S(2)}) async-start(bf16[8,8,2048]{2,1,0:T(8,128)(2,1)} %get-tuple-element.6), calls=%async_computation.3 | async-start | bytes 524288 | tf_op jit(solution)/shard_map/all_to_all | solution.py:148
Sparse Core Ops, SparseCore 0:
  23.2 30.4 reduce-scatter.2
  55.2 28.9 all-gather.2
  87.1 41.2 all-reduce.3
  140.9 28.6 reduce-scatter.4
  171.0 28.6 all-gather.4
  202.5 42.6 all-reduce.5
where the time goes:
time: 269 us; the launch traced here: 268 us
  waiting for transfers between devices  185 us (69%)
  blocking collectives  35.1 us (13%)
  matrix products  20.7 us (8%)
  between operations  13.8 us (5%)
  other arithmetic  6.95 us (3%)
  starting transfers between devices  4.98 us (2%)
    psum x1, waiting for transfers between devices, shards(): lax.psum(dense_terms.astype(jnp.bfloat16), 'tp').astype(jnp.float32)  42.8 us
    psum x1, waiting for transfers between devices, shards(): mixed_heads = lax.psum(head_terms, 'tp')  41.4 us
    all_gather x1, waiting for transfers between devices, shards(): lax.all_gather(dense_down_proj, 'ep', axis=1, tiled=True)  29.4 us
    reduce_scatter x1, waiting for transfers between devices, shards(): lax.psum_scatter(row_term(spread, joined), 'ep', scatter_dimension=0, til...  29.2 us
    all_gather x1, waiting for transfers between devices, shards(): lax.all_gather(output_weight, 'ep', axis=1, tiled=True)  22.4 us
    all_to_all x1, blocking collectives, shards(): lax.all_to_all(outbound, 'ep', split_axis=0, concat_axis=0, tiled=True)  12.7 us
    all_to_all x1, blocking collectives, shards(): lax.all_to_all(normed, 'ep', split_axis=1, concat_axis=0, tiled=True)  12.1 us
    all_to_all x1, blocking collectives, shards(): lax.all_to_all(ffn_in, 'ep', split_axis=1, concat_axis=0, tiled=True)  10.3 us
  transfers between devices with their start and end apart: 7, of which 7 were waited for; matrix products, arithmetic and copies ran while one was open for 6% of the time, Pallas kernels for 0%

commit v1 on v0

--- a/solution.py
+++ b/solution.py
@@ -103,7 +103,7 @@
     )
     attended = attended.reshape(seq_count, head_count * head_size)
     head_terms = right_product(attended, lax.all_gather(output_weight, "ep", axis=1, tiled=True))
-    mixed_heads = lax.psum(head_terms, "tp")
+    mixed_heads = jnp.sum(lax.all_gather(head_terms, "tp"), axis=0)
     residual = (tokens.astype(jnp.float32) + mixed_heads).astype(jnp.bfloat16)
     ffn_in = rms_scale(residual, ffn_gain).astype(jnp.bfloat16)
     dense_width = dense_gate_proj.shape[1]

time: 269 us -> 235 us (0.87)
  waiting for transfers between devices: 185 us -> 144 us
  blocking collectives: 35.1 us -> 44.3 us
    psum x1 -> x0, waiting for transfers between devices: 41.4 us -> none  [shards(): mixed_heads = lax.psum(head_terms, 'tp')]
    all_gather x0 -> x1, blocking collectives: none -> 10.1 us  [shards(): mixed_heads = jnp.sum(lax.all_gather(head_terms, 'tp'), axis=0)]
  transfers between devices with their start and end apart: 7 -> 6, of which waited for: 7 -> 6; matrix products, arithmetic and copies ran while one was open for 6% -> 7% of each run, Pallas kernels for 0% -> 0%
where the time goes in v1:
time: 235 us; the launch traced here: 234 us
  waiting for transfers between devices  144 us (61%)
  blocking collectives  44.3 us (19%)
  matrix products  20.2 us (9%)
  between operations  13.4 us (6%)
  other arithmetic  6.09 us (3%)
  starting transfers between devices  4.94 us (2%)
    psum x1, waiting for transfers between devices, shards(): lax.psum(dense_terms.astype(jnp.bfloat16), 'tp').astype(jnp.float32)  42.8 us
    all_gather x1, waiting for transfers between devices, shards(): lax.all_gather(dense_down_proj, 'ep', axis=1, tiled=True)  29.4 us
    reduce_scatter x1, waiting for transfers between devices, shards(): lax.psum_scatter(row_term(spread, joined), 'ep', scatter_dimension=0, til...  29.2 us
    all_gather x1, waiting for transfers between devices, shards(): lax.all_gather(output_weight, 'ep', axis=1, tiled=True)  22.4 us
    all_to_all x1, blocking collectives, shards(): lax.all_to_all(outbound, 'ep', split_axis=0, concat_axis=0, tiled=True)  12.7 us
    all_to_all x1, blocking collectives, shards(): lax.all_to_all(normed, 'ep', split_axis=1, concat_axis=0, tiled=True)  12.1 us
    all_gather x1, blocking collectives, shards(): mixed_heads = jnp.sum(lax.all_gather(head_terms, 'tp'), axis=0)  10.1 us
    all_to_all x1, waiting for transfers between devices, shards(): lax.all_to_all(expert_result.reshape(sources, slots_now, feature).astype(...  9.53 us
  transfers between devices with their start and end apart: 6, of which 6 were waited for; matrix products, arithmetic and copies ran while one was open for 7% of the time, Pallas kernels for 0%

profile of v1, /device:TPU:0, one launch (start us, length us, event | category | flops | bytes accessed | tf_op | source)
XLA Modules:
  0.0 234.4 jit_solution(15064704108632971363)
XLA Ops:
  6.5 0.0 copy-start
  6.5 0.0 reduce-scatter.3.cloned.1.call-start
  6.6 1.1 fusion.32
  7.7 0.9 fusion.34
  8.7 12.1 %all_to_all.48 = bf16[16,8,256]{2,0,1:T(8,128)(2,1)S(1)} all-to-all(bf16[16,8,256]{2,0,1:T(8,128)(2,1)S(1)} %bitcast.98), channel_id=1, replica_groups=mesh['ep'=8,'tp'=4] {'ep'}, dimensions={1} | all-to-all | bytes 131072 | tf_op jit(solution)/shard_map/all_to_all | solution.py:87
  20.7 2.3 fusion.20
  23.0 0.0 reduce-scatter.3.cloned.1.call-update
  23.0 0.0 all-gather.4.cloned.1.call-start
  23.1 0.7 all-gather.4.cloned.1.call-update
  23.8 0.0 reduce-scatter.5.cloned.1.call-start
  23.8 0.0 copy-done.10
  23.9 0.1 iota_compare_fusion
  23.9 0.0 copy-done.3
  23.9 0.1 select_reduce_fusion
  24.1 0.1 copy.42
  24.1 0.1 fusion.70
  24.3 0.1 copy.43
  24.4 0.1 iota_compare_fusion.1
  24.5 29.2 %reduce-scatter.3.cloned.1.call-done = f32[16,1536]{1,0:T(8,128)} async-done(((f32[128,1536]{1,0:T(8,128)}), f32[16,1536]{1,0:T(8,128)}) %reduce-scatter.3.cloned.1.call-update) | async-done | bytes 98320 | tf_op jit(solution)/shard_map/reduce_scatter | solution.py:89
  53.6 0.9 convert.8
  54.6 0.1 multiply_reduce_fusion
  54.7 0.0 copy-start.1
  54.7 5.2 %fusion.80 = f32[16,4,1,384]{3,2,1,0:T(1,128)S(1)} fusion(bf16[16,4,128,1]{2,3,1,0:T(2,128)(2,1)S(1)} %reshape.152, bf16[16,4,384,128]{3,2,1,0:T(8,128)(2,1)} %param.30), kind=kOutput, calls=%fused_computation.117 | convolution fusion | flops 6291456 | bytes 6406144 | tf_op jit(solution)/shard_map/shd,shpd->shp/dot_general | solution.py:28
  59.9 0.2 fusion.78
  60.1 0.2 fusion.50
  60.4 0.1 fusion.52
  60.5 1.2 fusion.48
  61.7 0.1 add_convert_fusion
  61.8 22.4 %all-gather.4.cloned.1.call-done = bf16[512,2048]{1,0:T(8,128)(2,1)} async-done(((bf16[512,256]{1,0:T(8,128)(2,1)}), bf16[512,2048]{1,0:T(8,128)(2,1)}) %all-gather.4.cloned.1.call-update) | async-done | bytes 2097168 | tf_op jit(solution)/shard_map/all_gather | solution.py:105
  84.2 2.0 fusion.55
  86.2 10.1 %all-gather = f32[64,2048]{1,0:T(8,128)S(1)} all-gather(f32[16,2048]{1,0:T(8,128)S(1)} %fusion.55), channel_id=2, replica_groups=mesh['ep'=8,'tp'=4] {'tp'}, dimensions={0}, use_global_device_ids=true | all-gather | bytes 655360 | tf_op jit(solution)/shard_map/all_gather | solution.py:106
  96.3 0.1 fusion.36
  96.5 0.0 copy-done.5
  96.5 0.1 fusion.38
  96.6 9.5 %all_to_all.49 = bf16[16,8,256]{2,0,1:T(8,128)(2,1)S(1)} all-to-all(bf16[16,8,256]{2,0,1:T(8,128)(2,1)S(1)} %bitcast.99), channel_id=1, replica_groups=mesh['ep'=8,'tp'=4] {'ep'}, dimensions={1} | all-to-all | bytes 131072 | tf_op jit(solution)/shard_map/all_to_all | solution.py:110
  106.1 0.9 convolution_convert_fusion.3
  107.0 0.0 reduce-scatter.5.cloned.1.call-update
  107.0 0.0 all-gather.6.cloned.1.call-start
  107.1 0.5 all-gather.6.cloned.1.call-update
  107.6 0.0 all-reduce.3.cloned.1.call-start
  107.7 0.1 copy.44
  107.8 0.1 eq.62
  107.8 0.1 fusion.59
  107.9 0.1 reduce_window_sum.11
  108.0 0.2 select_reduce_fusion.1
  108.2 0.1 reduce_sum.81
  108.2 0.1 copy.45
  108.3 0.3 fusion
  108.7 12.7 %all_to_all.50 = bf16[8,8,2048]{2,1,0:T(8,128)(2,1)S(1)} all-to-all(bf16[8,8,2048]{2,1,0:T(8,128)(2,1)S(1)} %fusion), channel_id=1, replica_groups=mesh['ep'=8,'tp'=4] {'ep'}, dimensions={0} | all-to-all | bytes 524288 | tf_op jit(solution)/shard_map/all_to_all | solution.py:140
  121.4 2.1 fusion.5
  123.5 3.2 %fusion.1 = bf16[8,8,2048]{2,1,0:T(8,128)(2,1)} fusion(bf16[1,512,2048]{2,1,0:T(8,128)(2,1)S(1)} %copy-done, bf16[1,2048,512]{2,1,0:T(8,128)(2,1)} %param.44, bf16[8,8,2048]{2,1,0:T(8,128)(2,1)S(1)} %all_to_all.50, f32[64,512]{1,0:T(8,128)S(1)} %fusion.5), kind=kOutput, calls=%fused_computation.5 | convolution fusion | flops 268763136 | bytes 4849664 | tf_op jit(solution)/shard_map/dot_general | solution.py:146
  126.7 9.0 %reduce-scatter.5.cloned.1.call-done = bf16[16,1024]{1,0:T(8,128)(2,1)} async-done(((bf16[128,1024]{1,0:T(8,128)(2,1)}), bf16[16,1024]{1,0:T(8,128)(2,1)}) %reduce-scatter.5.cloned.1.call-update) | async-done | bytes 32784 | tf_op jit(solution)/shard_map/reduce_scatter | solution.py:112
  135.8 0.8 convert_element_type.119
  136.5 29.4 %all-gather.6.cloned.1.call-done = bf16[512,2048]{1,0:T(8,128)(2,1)} async-done(((bf16[512,256]{1,0:T(8,128)(2,1)}), bf16[512,2048]{1,0:T(8,128)(2,1)}) %all-gather.6.cloned.1.call-update) | async-done | bytes 2097168 | tf_op jit(solution)/shard_map/all_gather | solution.py:121
  165.9 2.6 %convolution_convert_fusion.2 = bf16[16,2048]{1,0:T(8,128)(2,1)} fusion(bf16[512,2048]{1,0:T(8,128)(2,1)} %all-gather.6.cloned.1.call-done, f32[16,1024]{1,0:T(8,128)S(1)} %convert_element_type.119), kind=kOutput, calls=%fused_computation.6 | convolution fusion | flops 33636352 | bytes 2228224 | tf_op jit(solution)/shard_map/dot_general | solution.py:54
  168.5 0.0 all-reduce.3.cloned.1.call-update
  168.6 42.8 %all-reduce.3.cloned.1.call-done = (bf16[16,2048]{1,0:T(8,128)(2,1)}, bf16[8,8,2048]{2,1,0:T(8,128)(2,1)}) async-done(((bf16[16,2048]{1,0:T(8,128)(2,1)}, bf16[8,8,2048]{2,1,0:T(8,128)(2,1)}), (bf16[16,2048]{1,0:T(8,128)(2,1)}, bf16[8,8,2048]{2,1,0:T(8,128)(2,1)})) %all-reduce.3.cloned.1.call-update) | async-done | bytes 327696 | tf_op jit(solution)/shard_map/psum | solution.py:123
  211.4 4.7 %all-to-all-start.2 = ((bf16[8,8,2048]{2,1,0:T(8,128)(2,1)}), bf16[8,8,2048]{2,1,0:T(8,128)(2,1)S(1)}, u32[]{:S(2)}, u32[]{:S(2)}) async-start(bf16[8,8,2048]{2,1,0:T(8,128)(2,1)} %get-tuple-element.6), calls=%async_computation.3 | async-start | bytes 524288 | tf_op jit(solution)/shard_map/all_to_all | solution.py:148
  216.2 0.0 copy-done.6
  216.2 0.1 fusion.17
  216.3 9.5 %all-to-all-done.2 = bf16[8,8,2048]{2,1,0:T(8,128)(2,1)S(1)} async-done(((bf16[8,8,2048]{2,1,0:T(8,128)(2,1)}), bf16[8,8,2048]{2,1,0:T(8,128)(2,1)S(1)}, u32[]{:S(2)}, u32[]{:S(2)}) %all-to-all-start.2) | async-done | bytes 262176 | tf_op jit(solution)/shard_map/all_to_all | solution.py:148
  225.9 0.6 gather_fusion
  226.5 0.6 gather_fusion.1
  227.1 0.7 fusion.39
  (45 shorter events, 0.3 us)
Async XLA Ops:
  6.5 116.9 %copy-start = (bf16[1,512,2048]{2,1,0:T(8,128)(2,1)S(1)}, bf16[1,512,2048]{2,1,0:T(8,128)(2,1)}, u32[]{:S(2)}) copy-start(bf16[1,512,2048]{2,1,0:T(8,128)(2,1)} %param.45) | copy-start | bytes 6291460
  6.5 17.3 %copy-start.10 = (s32[16]{0:T(128)S(1)}, s32[16]{0:T(128)}, u32[]{:S(2)}) copy-start(s32[16]{0:T(128)} %param.33) | copy-start | bytes 196
  6.5 17.4 %copy-start.3 = (f32[16,4,384]{2,1,0:T(4,128)S(1)}, f32[16,4,384]{2,1,0:T(4,128)}, u32[]{:S(2)}) copy-start(f32[16,4,384]{2,1,0:T(4,128)} %param.32) | copy-start | bytes 294916
  6.5 17.6 %copy-start.13 = (bf16[2048,4]{0,1:T(4,128)(2,1)S(1)}, bf16[2048,4]{0,1:T(4,128)(2,1)}, u32[]{:S(2)}) copy-start(bf16[2048,4]{0,1:T(4,128)(2,1)} %param.28) | copy-start | bytes 49156
  6.5 17.6 %copy-start.14 = (f32[4]{0:T(128)S(1)}, f32[4]{0:T(128)}, u32[]{:S(2)}) copy-start(f32[4]{0:T(128)} %param.29) | copy-start | bytes 52
  6.5 47.1 %reduce-scatter.3.cloned.1.call-start = ((), (), s32[]{:S(2)}) async-start(), calls=%async_computation.6 | async-start | bytes 884736 | tf_op jit(solution)/shard_map/reduce_scatter | solution.py:89
  23.0 61.2 %all-gather.4.cloned.1.call-start = ((), (), s32[]{:S(2)}) async-start(), calls=%async_computation.7 | async-start | bytes 2359296 | tf_op jit(solution)/shard_map/all_gather | solution.py:105
  23.8 112.0 %reduce-scatter.5.cloned.1.call-start = ((), (), s32[]{:S(2)}) async-start(), calls=%async_computation.8 | async-start | bytes 294912 | tf_op jit(solution)/shard_map/reduce_scatter | solution.py:112
  54.7 5.8 %copy-start.1 = (bf16[16,4,384,128]{3,2,1,0:T(8,128)(2,1)S(1)}, bf16[16,4,384,128]{3,2,1,0:T(8,128)(2,1)}, u32[]{:S(2)}) copy-start(bf16[16,4,384,128]{3,2,1,0:T(8,128)(2,1)} %param.31) | copy-start | bytes 18874372
  61.7 34.7 %copy-start.2 = (bf16[16,2048]{1,0:T(8,128)(2,1)S(1)}, bf16[16,2048]{1,0:T(8,128)(2,1)}, u32[]{:S(2)}) copy-start(bf16[16,2048]{1,0:T(8,128)(2,1)} %param.23) | copy-start | bytes 196612
  61.7 34.8 %copy-start.5 = (f32[2048]{0:T(1024)S(1)}, f32[2048]{0:T(1024)}, u32[]{:S(2)}) copy-start(f32[2048]{0:T(1024)} %param.35) | copy-start | bytes 24580
  84.2 21.9 %copy-start.11 = (bf16[256,512]{1,0:T(8,128)(2,1)S(1)}, bf16[256,512]{1,0:T(8,128)(2,1)}, u32[]{:S(2)}) copy-start(bf16[256,512]{1,0:T(8,128)(2,1)} %param.37) | copy-start | bytes 786436
  84.2 21.9 %copy-start.12 = (bf16[256,512]{1,0:T(8,128)(2,1)S(1)}, bf16[256,512]{1,0:T(8,128)(2,1)}, u32[]{:S(2)}) copy-start(bf16[256,512]{1,0:T(8,128)(2,1)} %param.36) | copy-start | bytes 786436
  86.2 21.4 %copy-start.7 = (s32[16,2]{0,1:T(2,128)S(1)}, s32[16,2]{0,1:T(2,128)}, u32[]{:S(2)}) copy-start(s32[16,2]{0,1:T(2,128)} %param.40) | copy-start | bytes 388
  107.0 58.9 %all-gather.6.cloned.1.call-start = ((), (), s32[]{:S(2)}) async-start(), calls=%async_computation.9 | async-start | bytes 2359296 | tf_op jit(solution)/shard_map/all_gather | solution.py:121
  107.6 103.8 %all-reduce.3.cloned.1.call-start = ((), (), s32[]{:S(2)}) async-start(), calls=%async_computation.10 | async-start | bytes 655360 | tf_op jit(solution)/shard_map/psum | solution.py:123
  126.7 41.8 %copy-start.8 = (f32[16,2]{0,1:T(2,128)S(1)}, f32[16,2]{0,1:T(2,128)}, u32[]{:S(2)}) copy-start(f32[16,2]{0,1:T(2,128)} %param.42) | copy-start | bytes 388
  126.7 41.9 %copy-start.9 = (f32[16]{0:T(128)S(1)}, f32[16]{0:T(128)}, u32[]{:S(2)}) copy-start(f32[16]{0:T(128)} %param.41) | copy-start | bytes 196
  126.7 89.4 %copy-start.6 = (bf16[2048]{0:T(1024)(128)(2,1)S(1)}, bf16[2048]{0:T(1024)(128)(2,1)}, u32[]{:S(2)}) copy-start(bf16[2048]{0:T(1024)(128)(2,1)} %param.39) | copy-start | bytes 12292
  211.4 15.7 %copy-start.4 = (bf16[16,2048]{1,0:T(8,128)(2,1)S(1)}, bf16[16,2048]{1,0:T(8,128)(2,1)}, u32[]{:S(2)}) copy-start(bf16[16,2048]{1,0:T(8,128)(2,1)} %get-tuple-element.5) | copy-start | bytes 196612
  211.4 14.4 %all-to-all-start.2 = ((bf16[8,8,2048]{2,1,0:T(8,128)(2,1)}), bf16[8,8,2048]{2,1,0:T(8,128)(2,1)S(1)}, u32[]{:S(2)}, u32[]{:S(2)}) async-start(bf16[8,8,2048]{2,1,0:T(8,128)(2,1)} %get-tuple-element.6), calls=%async_computation.3 | async-start | bytes 524288 | tf_op jit(solution)/shard_map/all_to_all | solution.py:148
Sparse Core Ops, SparseCore 0:
  23.2 30.4 reduce-scatter.2
  55.2 28.9 all-gather.3
  107.2 28.5 reduce-scatter.4
  137.2 28.6 all-gather.5
  168.8 42.6 all-reduce.2
